TPU v7x, 512 devices: a whole 4x8x8 slice. The times are simulated.
512 devices in a mesh: kv: 64 (over z, y), tp: 8 (over x, core).
Axes of the slice: x: 4, y: 8, z: 8, core: 2. Of those that a mesh axis runs over, the one named last changes fastest.
Arguments:
- tokens: bfloat16 [512, 2048], P(None, ('kv', 'tp')), may hold values from -16 to 16
- mix_gain: float32 [2048], P('kv'), may hold values from 0.1 to 1.9
- query_weight: bfloat16 [2048, 2048], P('kv', 'tp'), may hold values from -0.125 to 0.125
- key_weight: bfloat16 [2048, 2048], P('kv', 'tp'), may hold values from -0.125 to 0.125
- value_weight: bfloat16 [2048, 2048], P('kv', 'tp'), may hold values from -0.125 to 0.125
- beta_weight: bfloat16 [2048, 16], P('kv', 'tp'), may hold values from -0.125 to 0.125
- decay_weight: bfloat16 [2048, 16], P('kv', 'tp'), may hold values from -0.125 to 0.125
- decay_rate: float32 [16], P('tp'), may hold values from 0.05 to 1
- prior_state: float32 [512, 16, 128, 128], P('kv', 'tp'), may hold values from -1.5 to 1.5
- tail_keys: bfloat16 [512, 16, 64, 128], P('kv', 'tp'), may hold values from -6 to 6
- tail_values: bfloat16 [512, 16, 64, 128], P('kv', 'tp'), may hold values from -6 to 6
- tail_beta: float32 [512, 16, 64], P('kv', 'tp'), may hold values from 0.1 to 0.9
- tail_decay: float32 [512, 16, 64], P('kv', 'tp'), may hold values from -2 to 0
- lengths: int32 [512], P('kv'), may hold values from 1 to 64, 13107 in all
- out_weight: bfloat16 [2048, 2048], P('tp', 'kv'), may hold values from -0.375 to 0.375
- mlp_gain: float32 [2048], P('kv'), may hold values from 0.1 to 1.9
- up_weight: bfloat16 [2048, 8192], P('kv', 'tp'), may hold values from -0.125 to 0.125
- down_weight: bfloat16 [8192, 2048], P('tp', 'kv'), may hold values from -0.0625 to 0.0625
Outputs:
- mixed: bfloat16 [512, 2048], P(None, ('kv', 'tp'))
All inputs are finite; a program needn't handle non-finite values. No bound on the sum of `lengths` on one device may be relied on, other than what follows from the above.
Results may differ from a plain program's by a relative error of at most 0.013.
Values may be sent and summed in bfloat16 or wider, within the bound.
A program may use at most 64 MiB of HBM per device.

v0:
```python
import jax
import jax.numpy as jnp
from jax import lax
from jax.sharding import Mesh
from jax.sharding import PartitionSpec as P

D = 2048
KV = ("kv_0", "kv_1")
KV_TP = ("kv_0", "kv_1", "tp")


epsilon = 1e-06


def in_order(parts, dim):
    dims = list(parts.shape[1:])
    dims[dim] *= parts.shape[0]
    return jnp.moveaxis(parts, 0, dim).reshape(dims)


def sent_to_all(value, axis):
    copies = jnp.broadcast_to(value, (lax.axis_size(axis), *value.shape))
    return lax.all_to_all(copies, axis, split_axis=0, concat_axis=0, tiled=True)


def gather_directly(value, axis, dim):
    return in_order(sent_to_all(value, axis), dim)


def cut_along(value, dim, devices):
    dims = value.shape
    parts = value.reshape(*dims[:dim], devices, dims[dim] // devices, *dims[dim + 1 :])
    return jnp.moveaxis(parts, dim, 0)


def sum_at_owner(value, axis, dim):
    parts = cut_along(value, dim, lax.axis_size(axis))
    arrived = lax.all_to_all(parts, axis, split_axis=0, concat_axis=0, tiled=True)
    return arrived.sum(axis=0)


def in_one_piece(arrays, axis, dim, along):
    columns = [a.reshape(*a.shape[:along], -1) for a in arrays]
    both = jnp.concatenate(columns, axis=along)
    out, at, done = (sum_at_owner(both, axis, dim), 0, [])
    for a, column in zip(arrays, columns):
        slab = out[..., at : at + column.shape[along]]
        done.append(slab.reshape(*slab.shape[:along], *a.shape[along:]))
        at += column.shape[along]
    return tuple(done)


def summed_rows(value, axes, dim):
    far, near = axes
    own = sum_at_owner(cut_along(value, dim, lax.axis_size(far)), near, dim + 1)
    return jnp.sum(lax.all_to_all(own, far, 0, 0, tiled=True), axis=0)


def side_by_side(arrays, axis, dim, along):
    columns = [a.reshape(*a.shape[:along], -1) for a in arrays]
    both = jnp.concatenate(columns, axis=along)
    out, at, done = (summed_rows(both, axis, dim), 0, [])
    for a, column in zip(arrays, columns):
        slab = out[..., at : at + column.shape[along]]
        done.append(slab.reshape(*slab.shape[:along], *a.shape[along:]))
        at += column.shape[along]
    return tuple(done)


def sum_at_owner_2(value, axis, dim):
    devices = lax.axis_size(axis)
    parts = lax.all_to_all(cut_along(value, dim, devices), axis, 0, 0, tiled=True)
    return jnp.sum(parts.astype(jnp.float32), axis=0)


def unit_rows(vectors):
    return vectors * lax.rsqrt(jnp.sum(vectors * vectors, axis=-1, keepdims=True) + epsilon)


def delta_read(
    previous_state,
    keys,
    value_vectors,
    betas,
    decays,
    live_count,
    queries,
    new_key,
    new_value,
    new_beta,
    new_decay,
):
    peak_value = lax.Precision.HIGHEST
    positions = keys.shape[1]
    head_dim = keys.shape[2]
    live_mask = jnp.arange(positions, dtype=jnp.int32)[None, :] < live_count[:, None]
    unit_keys = unit_rows(keys.astype(jnp.float32))
    value_rows = value_vectors.astype(jnp.float32)
    beta_live = jnp.where(live_mask, betas, 0.0)
    decay_live = jnp.where(live_mask, decays, 0.0)
    cumulative = jnp.cumsum(decay_live, axis=1)
    row_index = jnp.arange(positions, dtype=jnp.int32)
    strict = (row_index[:, None] > row_index[None, :])[None]
    log_gap = cumulative[:, :, None] - cumulative[:, None, :]
    key_intersection = jnp.einsum("nik,njk->nij", unit_keys, unit_keys, precision=peak_value)
    lower_part = jnp.where(
        strict,
        beta_live[:, :, None] * jnp.exp(jnp.where(strict, log_gap, 0.0)) * key_intersection,
        0.0,
    )
    system = lower_part + jnp.eye(positions, dtype=jnp.float32)[None]
    right_sides = jnp.concatenate(
        [
            (beta_live * jnp.exp(cumulative))[:, :, None] * unit_keys,
            beta_live[:, :, None] * value_rows,
        ],
        axis=2,
    )
    solved = jax.scipy.linalg.solve_triangular(system, right_sides, lower=True, unit_diagonal=True)
    weight_matrix_rows = solved[:, :, :head_dim]
    unscaled_rows = solved[:, :, head_dim:]
    adjusted_result = unscaled_rows - jnp.einsum(
        "mfd,mdx->mfx", weight_matrix_rows, previous_state, precision=peak_value
    )
    intersection = jnp.sum(new_key * queries, axis=1)
    test_vector = queries - (new_beta * intersection)[:, None] * new_key
    total_decay = cumulative[:, -1]
    state_readout = jnp.einsum("rq,rqt->rt", test_vector, previous_state, precision=peak_value)
    tail_weights = jnp.exp(total_decay[:, None] - cumulative) * jnp.einsum(
        "njk,nk->nj", unit_keys, test_vector, precision=peak_value
    )
    from_tail = jnp.einsum("nj,njv->nv", tail_weights, adjusted_result, precision=peak_value)
    readout = jnp.exp(total_decay)[:, None] * state_readout + from_tail
    return jnp.exp(new_decay)[:, None] * readout + (new_beta * intersection)[:, None] * new_value


def local(
    tokens,
    mix_gain,
    query_weight,
    key_weight,
    value_weight,
    beta_weight,
    decay_weight,
    decay_rate,
    prior_state,
    tail_keys,
    tail_values,
    tail_beta,
    tail_decay,
    lengths,
    out_weight,
    mlp_gain,
    up_weight,
    down_weight,
):
    own_rows = prior_state.shape[0]
    heads_here = prior_state.shape[1]
    head_dim = prior_state.shape[2]
    tail_span = tail_keys.shape[2]
    token_rows = gather_directly(tokens, "tp", 1)
    token_float = token_rows.astype(jnp.float32)
    square_part = jnp.sum(token_float * token_float, axis=1)
    normed = (token_float * mix_gain[None, :]).astype(jnp.bfloat16)
    query_part = jnp.dot(normed, query_weight, preferred_element_type=jnp.float32)
    key_part = jnp.dot(normed, key_weight, preferred_element_type=jnp.float32)
    value_part = jnp.dot(normed, value_weight, preferred_element_type=jnp.float32)
    beta_part = jnp.dot(normed, beta_weight, preferred_element_type=jnp.float32)
    decay_part = jnp.dot(normed, decay_weight, preferred_element_type=jnp.float32)
    summed = in_one_piece(
        (query_part, key_part, value_part, beta_part, decay_part, square_part), KV, 0, 1
    )
    own_squares = summed[5]
    row_scale = lax.rsqrt(own_squares / D + epsilon)[:, None]

    def by_heads(raw):
        return raw.reshape(own_rows, heads_here, head_dim)

    queries = unit_rows(jax.nn.silu(by_heads(summed[0] * row_scale)))
    new_keys = unit_rows(jax.nn.silu(by_heads(summed[1] * row_scale)))
    new_values = jax.nn.silu(by_heads(summed[2] * row_scale))
    new_beta = jax.nn.sigmoid(summed[3] * row_scale)
    new_decay = -decay_rate[None, :] * jax.nn.softplus(summed[4] * row_scale)
    count = own_rows * heads_here
    readout = delta_read(
        prior_state.reshape(count, head_dim, head_dim),
        tail_keys.reshape(count, tail_span, head_dim),
        tail_values.reshape(count, tail_span, head_dim),
        tail_beta.reshape(count, tail_span),
        tail_decay.reshape(count, tail_span),
        jnp.repeat(lengths, heads_here),
        queries.reshape(count, head_dim),
        new_keys.reshape(count, head_dim),
        new_values.reshape(count, head_dim),
        new_beta.reshape(count),
        new_decay.reshape(count),
    )
    head_out = readout.reshape(own_rows, heads_here * head_dim).astype(jnp.bfloat16)
    attended_block = jnp.dot(
        gather_directly(head_out, KV, 0), out_weight, preferred_element_type=jnp.float32
    )
    attended = sum_at_owner(attended_block, "tp", 1)
    mixed_in = (tokens.astype(jnp.float32) + attended).astype(jnp.bfloat16)
    mixer_rows = gather_directly(mixed_in, "tp", 1)
    mixer_float = mixer_rows.astype(jnp.float32)
    mixer_square_part = jnp.sum(mixer_float * mixer_float, axis=1)
    mixer_normed = (mixer_float * mlp_gain[None, :]).astype(jnp.bfloat16)
    up_part = jnp.dot(mixer_normed, up_weight, preferred_element_type=jnp.float32)
    up_own, own_mixer_squares = side_by_side((up_part, mixer_square_part), ("kv_0", "kv_1"), 0, 1)
    hidden_raw = up_own * lax.rsqrt(own_mixer_squares / D + epsilon)[:, None]
    hidden = jnp.square(jnp.maximum(hidden_raw, 0.0)).astype(jnp.bfloat16)
    down_block = jnp.dot(
        gather_directly(hidden, KV, 0), down_weight, preferred_element_type=jnp.float32
    )
    down = sum_at_owner_2(down_block.astype(jnp.bfloat16), "tp", 1)
    return (mixed_in.astype(jnp.float32) + down).astype(jnp.bfloat16)


def solution(mesh):
    split = Mesh(mesh.devices.reshape(8, 8, mesh.shape["tp"]), ("kv_0", "kv_1", "tp"))
    return jax.shard_map(
        local,
        mesh=split,
        in_specs=(
            P(None, KV_TP),
            P(KV),
            P(KV, "tp"),
            P(KV, "tp"),
            P(KV, "tp"),
            P(KV, "tp"),
            P(KV, "tp"),
            P("tp"),
            P(KV, "tp", None, None),
            P(KV, "tp", None, None),
            P(KV, "tp", None, None),
            P(KV, "tp", None),
            P(KV, "tp", None),
            P(KV),
            P("tp", KV),
            P(KV),
            P(KV, "tp"),
            P("tp", KV),
        ),
        out_specs=P(None, KV_TP),
        check_vma=False,
    )
```

profile of v0, /device:TPU:1, one launch (start us, length us, event | category | flops | bytes accessed | tf_op | source)
XLA Modules:
  0.0 290.9 jit_solution(930621850618314630)
XLA Ops:
  0.0 0.8 broadcast_in_dim.33
  0.8 13.9 %all_to_all.45 = bf16[8,512,4]{1,2,0:T(4,128)(2,1)S(1)} all-to-all(bf16[8,512,4]{1,2,0:T(4,128)(2,1)S(1)} %broadcast_in_dim.33), channel_id=1, replica_groups=mesh['kv_0'=8,'kv_1'=8,'tp'=8] {'tp'}, dimensions={0} | all-to-all | bytes 65536 | tf_op jit(solution)/shard_map/all_to_all | solution.py:23
  17.5 1.6 concatenate.16
  19.1 12.8 %all-to-all-start.1 = ((f32[64,8,773]{2,1,0:T(8,128)}), f32[64,8,773]{2,1,0:T(8,128)S(1)}, u32[]{:S(2)}, u32[]{:S(2)}) async-start(f32[64,8,773]{2,1,0:T(8,128)} %concatenate.16), calls=%async_computation.1 | async-start | bytes 3670016 | tf_op jit(solution)/shard_map/all_to_all | solution.py:38
  32.8 2.3 broadcast_multiply_fusion
  35.1 0.8 copy-done.1
  35.9 1.8 fusion.4
  37.7 80.0 %custom-call.4 = f32[16,1,64,64]{2,3,1,0:T(8,128)} custom-call(f32[16,1,64,64]{3,2,1,0:T(8,128)} %fusion.4), custom_call_target="InvertDiagBlocksLowerTriangular" | custom-call | tf_op jit(solution)/shard_map/jit(_solve_triangular)/vmap()/triangular_solve | solution.py:119
  117.9 2.3 fusion.5
  120.2 1.9 convolution_subtract_fusion
  123.4 1.0 fusion.60
  124.4 0.9 fusion.61
  125.5 1.6 fusion.62
  127.2 0.7 broadcast_in_dim.65
  127.9 12.1 %all-to-all-start.2 = ((bf16[64,8,256]{2,1,0:T(8,128)(2,1)}), bf16[64,8,256]{2,1,0:T(8,128)(2,1)S(1)}, u32[]{:S(2)}, u32[]{:S(2)}) async-start(bf16[64,8,256]{2,1,0:T(8,128)(2,1)} %broadcast_in_dim.65), calls=%async_computation.2 | async-start | bytes 524288 | tf_op jit(solution)/shard_map/all_to_all | solution.py:23
  140.1 12.5 %all-to-all-done.2 = bf16[64,8,256]{2,1,0:T(8,128)(2,1)S(1)} async-done(((bf16[64,8,256]{2,1,0:T(8,128)(2,1)}), bf16[64,8,256]{2,1,0:T(8,128)(2,1)S(1)}, u32[]{:S(2)}, u32[]{:S(2)}) %all-to-all-start.2) | async-done | bytes 262176 | tf_op jit(solution)/shard_map/all_to_all | solution.py:23
  152.8 10.6 %all_to_all.46 = f32[8,512,4]{1,2,0:T(4,128)S(1)} all-to-all(f32[8,512,4]{1,2,0:T(4,128)S(1)} %copy.122), channel_id=1, replica_groups=mesh['kv_0'=8,'kv_1'=8,'tp'=8] {'tp'}, dimensions={0} | all-to-all | bytes 131072 | tf_op jit(solution)/shard_map/all_to_all | solution.py:38
  163.5 7.9 %all_to_all.47 = bf16[8,512,4]{1,2,0:T(4,128)(2,1)S(1)} all-to-all(bf16[8,512,4]{1,2,0:T(4,128)(2,1)S(1)} %broadcast_in_dim.66), channel_id=1, replica_groups=mesh['kv_0'=8,'kv_1'=8,'tp'=8] {'tp'}, dimensions={0} | all-to-all | bytes 65536 | tf_op jit(solution)/shard_map/all_to_all | solution.py:23
  173.6 57.9 %all_to_all.48 = f32[8,8,8,1025]{3,2,1,0:T(8,128)S(1)} all-to-all(f32[8,8,8,1025]{3,2,1,0:T(8,128)S(1)} %copy.125), channel_id=1, replica_groups=mesh['kv_0'=8,'kv_1'=8,'tp'=8] {'kv_1'}, dimensions={0} | all-to-all | bytes 4198400 | tf_op jit(solution)/shard_map/all_to_all | solution.py:38
  231.5 0.8 reduce_sum.107
  232.3 13.3 %all_to_all.49 = f32[8,8,1025]{2,1,0:T(8,128)S(1)} all-to-all(f32[8,8,1025]{2,1,0:T(8,128)} %reduce_sum.107), channel_id=1, replica_groups=mesh['kv_0'=8,'kv_1'=8,'tp'=8] {'kv_0'}, dimensions={0} | all-to-all | bytes 524800 | tf_op jit(solution)/shard_map/all_to_all | solution.py:56
  246.0 32.9 %all_to_all.50 = bf16[64,8,1024]{2,1,0:T(8,128)(2,1)S(1)} all-to-all(bf16[64,8,1024]{2,1,0:T(8,128)(2,1)S(1)} %broadcast_in_dim.67), channel_id=1, replica_groups=mesh['kv_0'=8,'kv_1'=8,'tp'=8] {'kv_0','kv_1'}, dimensions={0} | all-to-all | bytes 2097152 | tf_op jit(solution)/shard_map/all_to_all | solution.py:23
  279.3 10.9 %all_to_all.51 = bf16[8,512,4]{1,2,0:T(4,128)(2,1)S(1)} all-to-all(bf16[8,512,4]{1,2,0:T(4,128)(2,1)S(1)} %bitcast.119), channel_id=1, replica_groups=mesh['kv_0'=8,'kv_1'=8,'tp'=8] {'tp'}, dimensions={0} | all-to-all | bytes 65536 | tf_op jit(solution)/shard_map/all_to_all | solution.py:72
  290.3 0.6 add_convert_fusion
  (106 shorter events, 8.5 us)
Async XLA Ops:
  0.0 120.2 %copy-start = (f32[8,2,128,128]{3,2,1,0:T(8,128)S(1)}, f32[8,2,128,128]{3,2,1,0:T(8,128)}, u32[]{:S(2)}) copy-start(f32[8,2,128,128]{3,2,1,0:T(8,128)} %param.26) | copy-start | bytes 3145732
  0.0 16.0 %copy-start.13 = (f32[32]{0:T(128)S(1)}, f32[32]{0:T(128)}, u32[]{:S(2)}) copy-start(f32[32]{0:T(128)} %param.19) | copy-start | bytes 388
  0.0 16.2 %copy-start.14 = (bf16[32,2]{0,1:T(2,128)(2,1)S(1)}, bf16[32,2]{0,1:T(2,128)(2,1)}, u32[]{:S(2)}) copy-start(bf16[32,2]{0,1:T(2,128)(2,1)} %param.23) | copy-start | bytes 388
  0.0 16.3 %copy-start.15 = (bf16[32,2]{0,1:T(2,128)(2,1)S(1)}, bf16[32,2]{0,1:T(2,128)(2,1)}, u32[]{:S(2)}) copy-start(bf16[32,2]{0,1:T(2,128)(2,1)} %param.24) | copy-start | bytes 388
  0.0 16.8 %copy-start.8 = (bf16[32,256]{1,0:T(8,128)(2,1)S(1)}, bf16[32,256]{1,0:T(8,128)(2,1)}, u32[]{:S(2)}) copy-start(bf16[32,256]{1,0:T(8,128)(2,1)} %param.22) | copy-start | bytes 49156
  0.0 17.0 %copy-start.9 = (bf16[32,256]{1,0:T(8,128)(2,1)S(1)}, bf16[32,256]{1,0:T(8,128)(2,1)}, u32[]{:S(2)}) copy-start(bf16[32,256]{1,0:T(8,128)(2,1)} %param.21) | copy-start | bytes 49156
  15.0 2.2 copy-start.10
  19.0 12.9 %copy-start.18 = (f32[2]{0:T(128)S(1)}, f32[2]{0:T(128)}, u32[]{:S(2)}) copy-start(f32[2]{0:T(128)} %param.25) | copy-start | bytes 28
  19.0 12.9 %copy-start.16 = (s32[8]{0:T(128)S(1)}, s32[8]{0:T(128)}, u32[]{:S(2)}) copy-start(s32[8]{0:T(128)} %param.31) | copy-start | bytes 100
  19.0 13.1 %copy-start.11 = (f32[8,2,64]{2,1,0:T(2,128)S(1)}, f32[8,2,64]{2,1,0:T(2,128)}, u32[]{:S(2)}) copy-start(f32[8,2,64]{2,1,0:T(2,128)} %param.30) | copy-start | bytes 12292
  19.0 13.4 %copy-start.3 = (bf16[8,2,64,128]{3,2,1,0:T(8,128)(2,1)S(1)}, bf16[8,2,64,128]{3,2,1,0:T(8,128)(2,1)}, u32[]{:S(2)}) copy-start(bf16[8,2,64,128]{3,2,1,0:T(8,128)(2,1)} %param.27) | copy-start | bytes 786436
  19.0 13.7 %copy-start.12 = (f32[8,2,64]{2,1,0:T(2,128)S(1)}, f32[8,2,64]{2,1,0:T(2,128)}, u32[]{:S(2)}) copy-start(f32[8,2,64]{2,1,0:T(2,128)} %param.29) | copy-start | bytes 12292
  19.1 103.0 %all-to-all-start.1 = ((f32[64,8,773]{2,1,0:T(8,128)}), f32[64,8,773]{2,1,0:T(8,128)S(1)}, u32[]{:S(2)}, u32[]{:S(2)}) async-start(f32[64,8,773]{2,1,0:T(8,128)} %concatenate.16), calls=%async_computation.1 | async-start | bytes 3670016 | tf_op jit(solution)/shard_map/all_to_all | solution.py:38
  35.1 0.8 copy-start.1
  120.2 4.3 %copy-start.2 = (f32[16,64,128]{2,1,0:T(8,128)S(1)}, f32[16,64,128]{2,1,0:T(8,128)}, u32[]{:S(2)}) copy-start(f32[16,64,128]{2,1,0:T(8,128)} %copy-done.1) | copy-start | bytes 1572868
  122.1 18.0 %copy-start.6 = (bf16[256,32]{0,1:T(8,128)(2,1)S(1)}, bf16[256,32]{0,1:T(8,128)(2,1)}, u32[]{:S(2)}) copy-start(bf16[256,32]{0,1:T(8,128)(2,1)} %param.32) | copy-start | bytes 49156
  122.2 41.3 %copy-start.7 = (bf16[512,4]{0,1:T(4,128)(2,1)S(1)}, bf16[512,4]{0,1:T(4,128)(2,1)}, u32[]{:S(2)}) copy-start(bf16[512,4]{0,1:T(4,128)(2,1)} %param.18) | copy-start | bytes 12292
  127.1 45.7 %copy-start.5 = (bf16[32,1024]{1,0:T(8,128)(2,1)S(1)}, bf16[32,1024]{1,0:T(8,128)(2,1)}, u32[]{:S(2)}) copy-start(bf16[32,1024]{1,0:T(8,128)(2,1)} %param.34) | copy-start | bytes 196612
  127.1 45.7 %copy-start.17 = (f32[32]{0:T(128)S(1)}, f32[32]{0:T(128)}, u32[]{:S(2)}) copy-start(f32[32]{0:T(128)} %param.33) | copy-start | bytes 388
  127.9 24.6 %all-to-all-start.2 = ((bf16[64,8,256]{2,1,0:T(8,128)(2,1)}), bf16[64,8,256]{2,1,0:T(8,128)(2,1)S(1)}, u32[]{:S(2)}, u32[]{:S(2)}) async-start(bf16[64,8,256]{2,1,0:T(8,128)(2,1)} %broadcast_in_dim.65), calls=%async_computation.2 | async-start | bytes 524288 | tf_op jit(solution)/shard_map/all_to_all | solution.py:23
  232.3 46.6 %copy-start.4 = (bf16[1024,32]{0,1:T(8,128)(2,1)S(1)}, bf16[1024,32]{0,1:T(8,128)(2,1)}, u32[]{:S(2)}) copy-start(bf16[1024,32]{0,1:T(8,128)(2,1)} %param.35) | copy-start | bytes 196612
where the time goes:
time: 292 us; the launch traced here: 291 us
  blocking collectives  147 us (50%)
  other arithmetic  86.2 us (30%)
  starting transfers between devices  25 us (9%)
  waiting for transfers between devices  12.5 us (4%)
  matrix products  11.2 us (4%)
  local copies, waits for them, and re-layouts  8.17 us (3%)
    another operation x2, other arithmetic, delta_read(): jax.scipy.linalg.solve_triangular(system, right_sides, lower=True, unit_d...  80 us
    all_to_all x2, blocking collectives, sum_at_owner(): lax.all_to_all(parts, axis, split_axis=0, concat_axis=0, tiled=True)  68.5 us
    all_to_all x3, blocking collectives, sent_to_all(): return lax.all_to_all(copies, axis, split_axis=0, concat_axis=0, tiled=True)  54.7 us
    all_to_all x1, blocking collectives, summed_rows(): return jnp.sum(lax.all_to_all(own, far, 0, 0, tiled=True), axis=0)  13.3 us
    all_to_all x1, starting transfers between devices, sum_at_owner(): lax.all_to_all(parts, axis, split_axis=0, concat_axis=0, tiled=True)  12.8 us
    all_to_all x1, waiting for transfers between devices, sent_to_all(): return lax.all_to_all(copies, axis, split_axis=0, concat_axis=0, tiled=True)  12.5 us
    all_to_all x1, starting transfers between devices, sent_to_all(): return lax.all_to_all(copies, axis, split_axis=0, concat_axis=0, tiled=True)  12.1 us
    all_to_all x1, blocking collectives, sum_at_owner_2(): lax.all_to_all(cut_along(value, dim, devices), axis, 0, 0, tiled=True)  10.9 us
  transfers between devices with their start and end apart: 2, of which 1 were waited for; matrix products, arithmetic and copies ran while one was open for 31% of the time, Pallas kernels for 0%

commit v1 on v0

v1 whole, which is shorter than its diff:
```python
import jax
import jax.numpy as jnp
from jax import lax
from jax.experimental import pallas as pl
from jax.experimental.pallas import tpu as pltpu
from jax.sharding import PartitionSpec as P

D = 2048
N = 8
SEQ = 64
T_LEN = 64
epsilon = 1e-06
BF = jnp.bfloat16
F32 = jnp.float32
HI = lax.Precision.HIGHEST
MESH = pl.DeviceIdType.MESH

(TOK_A, TOK_B, W_Q, W_K, W_V, W_B, W_D, G_MIX, G_MLP, W_OUT, W_UP, W_DOWN,
 P_MAIN, P_AUX, HEADS, ATT, U_MAIN, U_AUX, HID, DOWN, FIN) = range(21)


def nt(a, b, precision=None):
    return lax.dot_general(a, b, (((1,), (1,)), ((), ())), preferred_element_type=F32, precision=precision)


def nn(a, b, precision=None):
    return lax.dot_general(a, b, (((1,), (0,)), ((), ())), preferred_element_type=F32, precision=precision)


def iota(shape, dim):
    return lax.broadcasted_iota(jnp.int32, shape, dim)


def split_rows(x):
    high = x.astype(BF)
    low = (x - high.astype(F32)).astype(BF)
    return jnp.concatenate([high.astype(F32), low.astype(F32)], axis=0).astype(BF)


def own_row(r):
    return jnp.sum(jnp.where(iota(r.shape, 0) == iota(r.shape, 1), r, 0.0), axis=0)


def rows_by(x, mats, contract):
    both = split_rows(x)
    lhs = jnp.broadcast_to(both[None], (N, *both.shape))
    r = lax.dot_general(lhs, mats, (((2,), (contract,)), ((0,), (0,))), preferred_element_type=F32)
    return own_row(r[:, :N] + r[:, N:])


def unit(x):
    return x * lax.rsqrt(jnp.sum(x * x, axis=-1, keepdims=True) + epsilon)


def silu(x):
    return x * (1.0 / (1.0 + jnp.exp(-x)))


def kernel(
    tok, mix_gain, wq, wk, wv, wb, wd, rate, state, tail_k, tail_v, tail_b, tail_g, lengths, wo, mlp_gain, wu, wdn,
    out,
    tok_a, x32, perm, xs, xt, xf, gq, gk, gv, gb, gd, ggm, ggl, go, gu, gdn, dperm, bd, gains,
    kbuf, vbuf, sbuf, sbf, tri, coef, pms, pmr, pxs, pxr, heads, att, mixed, mixt, ums, umr, uxs, uxr, hid, dns, dnr,
    fins, finr, flat, send_sem, recv_sem, local_sem,
):
    kv = lax.axis_index("kv")
    tp = lax.axis_index("tp")
    z = kv // N
    y = kv % N

    def peer(axis, r):
        if axis == "z":
            return (((z + r) % N) * N + y, tp)
        if axis == "y":
            return (z * N + (y + r) % N, tp)
        return (kv, (tp + r) % N)

    me = {"z": z, "y": y, "tp": tp}

    def copy(phase, axis, src, dst, r, slot, cut):
        return pltpu.make_async_remote_copy(
            src_ref=src.at[cut] if cut is not None else src,
            dst_ref=dst.at[slot],
            send_sem=send_sem.at[phase, r],
            recv_sem=recv_sem.at[phase, r],
            device_id=peer(axis, r),
            device_id_type=MESH,
        )

    plans = {}

    def send(phase, axis, src, dst, cut):
        plans[phase] = (axis, src, dst, cut)

        def step(r, _):
            where = (me[axis] + r) % N if cut == "peer" else (me[axis] if cut == "me" else None)
            copy(phase, axis, src, dst, r, me[axis], where).start()
            return 0

        lax.fori_loop(1, N, step, 0)

    def recv(phase):
        axis, src, dst, cut = plans[phase]

        def step(r, _):
            where = me[axis] if cut is not None else None
            copy(phase, axis, src, dst, r, (me[axis] - r + N) % N, where).wait_recv()
            return 0

        lax.fori_loop(1, N, step, 0)

    def sent(phase):
        axis, src, dst, cut = plans[phase]

        def step(r, _):
            where = me[axis] if cut is not None else None
            copy(phase, axis, src, dst, r, me[axis], where).wait_send()
            return 0

        lax.fori_loop(1, N, step, 0)

    loads = []
    for h in range(2):
        loads.append(pltpu.make_async_copy(tail_k.at[:, h], kbuf.at[h], local_sem.at[h]))
        loads.append(pltpu.make_async_copy(tail_v.at[:, h], vbuf.at[h], local_sem.at[2 + h]))
        loads.append(pltpu.make_async_copy(state.at[:, h], sbuf.at[h], local_sem.at[4 + h]))
    for load in loads:
        load.start()

    barrier = pltpu.get_barrier_semaphore()

    def greet(r, _):
        for axis in ("z", "y", "tp"):
            pl.semaphore_signal(barrier, inc=1, device_id=peer(axis, r), device_id_type=MESH)
        return 0

    lax.fori_loop(1, N, greet, 0)
    pl.semaphore_wait(barrier, 3 * (N - 1))

    send(TOK_A, "tp", tok, tok_a, None)
    send(G_MIX, "y", mix_gain, ggm, None)
    send(W_B, "y", wb, gb, None)
    send(W_D, "y", wd, gd, None)
    send(W_Q, "y", wq, gq, None)
    send(W_K, "y", wk, gk, None)

    tok_a[tp] = tok[...]
    ggm[y] = mix_gain[...]
    ggl[y] = mlp_gain[...]
    gb[y] = wb[...]
    gd[y] = wd[...]
    gq[y] = wq[...]
    gk[y] = wk[...]
    gv[y] = wv[...]
    go[y] = wo[...]
    gu[y] = wu[...]
    gdn[y] = wdn[...]
    bd[...] = jnp.zeros_like(bd)
    flat[...] = jnp.zeros_like(flat)
    row = iota((N * SEQ, N * SEQ), 0)
    column = iota((N * SEQ, N * SEQ), 1)
    swapped = (row // 64) * 8 + ((row // 8) % 8) * 64 + row % 8
    perm[...] = jnp.where(column == swapped, 1.0, 0.0).astype(BF)

    recv(TOK_A)
    for t in range(N):
        x32[4 * t : 4 * t + 4, :] = tok_a[t].astype(F32)
    arranged = nn(x32[...].astype(BF), perm[...])
    for t in range(N):
        xs[t] = arranged[:, 64 * t : 64 * t + 64].astype(BF)
    xt[y] = xs[y]
    send(TOK_B, "y", xs, xt, "peer")
    send(W_V, "y", wv, gv, None)
    send(G_MLP, "y", mlp_gain, ggl, None)
    send(W_OUT, "y", wo, go, None)
    send(W_UP, "y", wu, gu, None)
    send(W_DOWN, "y", wdn, gdn, None)

    for load in loads:
        load.wait()
    lens = jnp.zeros((N, T_LEN), jnp.int32)
    for i in range(N):
        lens = jnp.where(iota((N, T_LEN), 0) == i, lengths[i], lens)
    live = iota((N, T_LEN), 1) < lens
    upper = jnp.where(iota((T_LEN, T_LEN), 0) <= iota((T_LEN, T_LEN), 1), 1.0, 0.0)
    betas, gammas, totals, b3, g3, c3 = [], [], [], [], [], []
    for h in range(2):
        beta = jnp.where(live, tail_b[:, h, :], 0.0)
        decay = jnp.where(live, tail_g[:, h, :], 0.0)
        gamma = nn(decay, upper, HI)
        betas.append(beta)
        gammas.append(gamma)
        totals.append(jnp.sum(decay, axis=1, keepdims=True))
        b3.append(beta[:, None, :])
        g3.append(decay[:, None, :])
        c3.append(gamma[:, None, :])
    b3 = jnp.concatenate(b3, axis=0)
    g3 = jnp.concatenate(g3, axis=0)
    c3 = jnp.concatenate(c3, axis=0)
    keys = kbuf[...].reshape(2 * N, T_LEN, 128)
    gram = lax.dot_general(keys, keys, (((2,), (2,)), ((0,), (0,))), preferred_element_type=F32)
    i0 = iota((2 * N, T_LEN, T_LEN), 1)
    j0 = iota((2 * N, T_LEN, T_LEN), 2)
    diagonal = jnp.where(i0 == j0, gram, 0.0)
    inv_row = lax.rsqrt(jnp.sum(diagonal, axis=1, keepdims=True) + epsilon)
    inv_col = lax.rsqrt(jnp.sum(diagonal, axis=2, keepdims=True) + epsilon)
    gamma_col = jnp.sum(jnp.where(j0 <= i0, g3, 0.0), axis=2, keepdims=True)
    beta_col = jnp.sum(jnp.where(j0 == i0, b3, 0.0), axis=2, keepdims=True)
    below = i0 > j0
    lower = jnp.where(
        below, beta_col * jnp.exp(jnp.where(below, gamma_col - c3, 0.0)) * gram * inv_col * inv_row, 0.0
    )

    def part(m):
        return jnp.where((i0 // (2 * m) == j0 // (2 * m)) & (i0 // m != j0 // m), lower, 0.0)

    def bmm(a, b):
        return lax.dot_general(a, b, (((2,), (1,)), ((0,), (0,))), preferred_element_type=F32, precision=HI)

    inverse = jnp.where(i0 == j0, 1.0, 0.0) - part(1)
    for m in (2, 4, 8, 16, 32):
        inverse = inverse - bmm(bmm(inverse, part(m)), inverse)
    tri[...] = inverse
    for n in range(2 * N):
        coef[n : n + 1, :] = inv_row[n]
    sbf[...] = sbuf[...].astype(BF)

    for phase in (G_MIX, W_B, W_D, TOK_B):
        recv(phase)
    for t in range(N):
        gains[0:1, 32 * t : 32 * t + 32] = ggm[t]
        bd[0:2, 32 * t : 32 * t + 32] = gb[t].astype(F32)
        bd[2:4, 32 * t : 32 * t + 32] = gd[t].astype(F32)
    eye64 = jnp.where(iota((SEQ, SEQ), 0) == iota((SEQ, SEQ), 1), 1.0, 0.0).astype(BF)
    token = nt(eye64, xt[...].reshape(256, SEQ))
    xf[...] = token
    squares = jnp.sum(token * token, axis=1, keepdims=True)
    normed = (token * gains[0:1, :]).astype(BF)
    aux = nt(normed, bd[...].astype(BF))
    pxs[...] = jnp.where(iota((SEQ, 128), 1) == 4, squares, aux).reshape(N, N, 128)
    pxr[z] = pxs[z]
    send(P_AUX, "z", pxs, pxr, "peer")
    for at, (phase, w) in enumerate(((W_Q, gq), (W_K, gk), (W_V, gv))):
        recv(phase)
        pms[:, :, 256 * at : 256 * at + 256] = (
            nn(normed, w[...].reshape(256, 256)).reshape(N, N, 256).astype(BF)
        )
    pmr[z] = pms[z]
    send(P_MAIN, "z", pms, pmr, "peer")

    recv(P_AUX)
    aux = jnp.sum(pxr[...], axis=0)
    row_scale = lax.rsqrt(aux[:, 4:5] / D + epsilon)
    recv(P_MAIN)
    raw = jnp.sum(pmr[...].astype(F32), axis=0) * row_scale
    results = []
    for h in range(2):
        query = unit(silu(raw[:, 128 * h : 128 * h + 128]))
        key = unit(silu(raw[:, 256 + 128 * h : 384 + 128 * h]))
        value = silu(raw[:, 512 + 128 * h : 640 + 128 * h])
        new_beta = 1.0 / (1.0 + jnp.exp(-(aux[:, h : h + 1] * row_scale)))
        pre = aux[:, 2 + h : 3 + h] * row_scale
        soft = jnp.maximum(pre, 0.0) + jnp.log(1.0 + jnp.exp(-jnp.abs(pre)))
        new_decay = -rate[h] * soft
        weight = new_beta * jnp.sum(key * query, axis=1, keepdims=True)
        test = query - weight * key
        inv = coef[N * h : N * h + N, :]
        a = rows_by(test, kbuf[h], 2) * jnp.exp(totals[h] - gammas[h]) * inv
        lhs = jnp.broadcast_to(a[None], (N, N, T_LEN))
        solved = own_row(bmm(lhs, tri[N * h : N * h + N])) * betas[h]
        from_values = rows_by(solved, vbuf[h], 1)
        moved = jnp.exp(totals[h]) * test - rows_by(solved * jnp.exp(gammas[h]) * inv, kbuf[h], 1)
        readout = rows_by(moved, sbf[h], 1) + from_values
        results.append(jnp.exp(new_decay) * readout + weight * value)
    heads[z] = jnp.concatenate(results, axis=1).astype(BF)
    send(HEADS, "z", heads, heads, "me")

    recv(W_OUT)
    recv(G_MLP)
    for t in range(N):
        gains[1:2, 32 * t : 32 * t + 32] = ggl[t]
    recv(HEADS)
    gathered = heads[...].astype(F32).reshape(SEQ, 256).astype(BF)
    att[tp] = nt(gathered, go[...].reshape(256, 256)).astype(BF)
    send(ATT, "tp", att, att, "me")
    r0 = iota((256, 256), 0)
    r1 = iota((256, 256), 1)
    regroup = jnp.where(r1 == ((r0 // 4) % 8) * 32 + (r0 // 32) * 4 + r0 % 4, 1.0, 0.0).astype(BF)
    recv(W_UP)
    recv(ATT)
    mixed[...] = (xf[...] + jnp.sum(att[...].astype(F32), axis=0)).astype(BF)
    mixer = mixed[...].astype(F32)
    squares = jnp.sum(mixer * mixer, axis=1, keepdims=True)
    uxs[...] = jnp.broadcast_to(squares, (SEQ, 128)).reshape(N, N, 128)
    uxr[z] = uxs[z]
    send(U_AUX, "z", uxs, uxr, "peer")
    normed = (mixer * gains[1:2, :]).astype(BF)
    ums[...] = nn(normed, gu[...].reshape(256, 1024)).reshape(N, N, 1024).astype(BF)
    umr[z] = ums[z]
    send(U_MAIN, "z", ums, umr, "peer")
    mixt[...] = nt(regroup, mixed[...]).reshape(N, 32, SEQ)
    recv(U_AUX)
    row_scale = lax.rsqrt(jnp.sum(uxr[...], axis=0)[:, 0:1] / D + epsilon)
    recv(U_MAIN)
    raw = jnp.maximum(jnp.sum(umr[...].astype(F32), axis=0) * row_scale, 0.0)
    hid[z] = (raw * raw).astype(BF)
    send(HID, "z", hid, hid, "me")
    recv(W_DOWN)
    dperm[...] = nn(regroup, gdn[...].reshape(256, 1024)).astype(BF)
    recv(HID)
    hidden = hid[...].astype(F32).reshape(SEQ, 1024).astype(BF)
    dns[...] = nt(dperm[...], hidden).reshape(N, 32, SEQ).astype(BF)
    dnr[tp] = dns[tp]
    send(DOWN, "tp", dns, dnr, "peer")
    recv(DOWN)
    total = mixt[tp] + jnp.sum(dnr[...].astype(F32), axis=0)
    for t in range(N):
        fins[t] = total[4 * t : 4 * t + 4, :].astype(BF)
    finr[y] = fins[y]
    send(FIN, "y", fins, finr, "peer")
    recv(FIN)
    for t in range(N):
        flat[0:4, 64 * t : 64 * t + 64] = finr[t].astype(F32)
    out[...] = nn(flat[...].astype(BF), perm[...])[0:4, :].astype(BF)
    for phase in sorted(plans):
        sent(phase)


def local(
    tokens, mix_gain, query_weight, key_weight, value_weight, beta_weight, decay_weight, decay_rate, prior_state,
    tail_keys, tail_values, tail_beta, tail_decay, lengths, out_weight, mlp_gain, up_weight, down_weight,
):
    vmem = pl.BlockSpec(memory_space=pltpu.VMEM)
    smem = pl.BlockSpec(memory_space=pltpu.SMEM)
    hbm = pl.BlockSpec(memory_space=pl.ANY)
    specs = [vmem] * 7 + [smem] + [hbm] * 3 + [vmem] * 2 + [smem] + [vmem] * 4

    def v(*shape, dtype=BF):
        return pltpu.VMEM(shape, dtype)

    result = pl.pallas_call(
        kernel,
        out_shape=jax.ShapeDtypeStruct((4, 512), BF),
        in_specs=specs,
        out_specs=vmem,
        scratch_shapes=[
            v(8, 4, 512), v(32, 512, dtype=F32), v(512, 512), v(8, 32, 64), v(8, 32, 64), v(64, 256, dtype=F32),
            v(8, 32, 256), v(8, 32, 256), v(8, 32, 256), v(8, 2, 32), v(8, 2, 32),
            v(8, 1, 32, dtype=F32), v(8, 1, 32, dtype=F32),
            v(8, 32, 256), v(8, 32, 1024), v(8, 32, 1024), v(256, 1024), v(128, 256, dtype=F32), v(8, 256, dtype=F32),
            v(2, 8, 64, 128), v(2, 8, 64, 128), v(2, 8, 128, 128, dtype=F32), v(2, 8, 128, 128),
            v(16, 64, 64, dtype=F32), v(16, 64, dtype=F32),
            v(8, 8, 768), v(8, 8, 768), v(8, 8, 128, dtype=F32), v(8, 8, 128, dtype=F32),
            v(8, 8, 256), v(8, 64, 256), v(64, 256), v(8, 32, 64, dtype=F32),
            v(8, 8, 1024), v(8, 8, 1024), v(8, 8, 128, dtype=F32), v(8, 8, 128, dtype=F32),
            v(8, 8, 1024), v(8, 32, 64), v(8, 32, 64), v(8, 4, 64), v(8, 4, 64), v(8, 512, dtype=F32),
            pltpu.SemaphoreType.DMA((21, 8)), pltpu.SemaphoreType.DMA((21, 8)), pltpu.SemaphoreType.DMA((6,)),
        ],
        compiler_params=pltpu.CompilerParams(collective_id=0, has_side_effects=True),
    )(
        tokens.T, mix_gain.reshape(1, -1), query_weight, key_weight, value_weight, beta_weight.T, decay_weight.T,
        decay_rate, prior_state, tail_keys, tail_values, tail_beta, tail_decay, lengths, out_weight.T,
        mlp_gain.reshape(1, -1), up_weight, down_weight.T,
    )
    return result.T


def solution(mesh):
    kt = ("kv", "tp")
    return jax.shard_map(
        local,
        mesh=mesh,
        in_specs=(
            P(None, kt), P("kv"), P("kv", "tp"), P("kv", "tp"), P("kv", "tp"), P("kv", "tp"), P("kv", "tp"), P("tp"),
            P("kv", "tp", None, None), P("kv", "tp", None, None), P("kv", "tp", None, None),
            P("kv", "tp", None), P("kv", "tp", None), P("kv"), P("tp", "kv"), P("kv"), P("kv", "tp"), P("tp", "kv"),
        ),
        out_specs=P(None, kt),
        check_vma=False,
    )
```

time: 292 us -> 73.9 us (0.25)
  blocking collectives: 147 us -> 0 us
  other arithmetic: 86.2 us -> 0 us
  Pallas kernels: 0 us -> 72.4 us
  starting transfers between devices: 25 us -> 0 us
  waiting for transfers between devices: 12.5 us -> 0 us
  matrix products: 11.2 us -> 0 us
  local copies, waits for them, and re-layouts: 8.17 us -> 1.28 us
    all_to_all x7 -> x0, blocking collectives: 147 us -> none  [the longest x2 68.5 us: sum_at_owner(): lax.all_to_all(parts, axis, split_axis=0, concat_axis=0, tiled=True)]
    another operation x3 -> x0, other arithmetic: 80.2 us -> none  [the longest x2 80 us: delta_read(): jax.scipy.linalg.solve_triangular(system, right_sides, lower=True, unit_d...]
    pallas_call x0 -> x1, Pallas kernels: none -> 72.4 us  [local(): pl.pallas_call(kernel, out_shape=jax.ShapeDtypeStruct((4, 512), BF), in_s...]
    all_to_all x2 -> x0, starting transfers between devices: 25 us -> none  [the longest x1 12.8 us: sum_at_owner(): lax.all_to_all(parts, axis, split_axis=0, concat_axis=0, tiled=True)]
    all_to_all x2 -> x0, waiting for transfers between devices: 12.5 us -> none  [the longest x1 12.5 us: sent_to_all(): return lax.all_to_all(copies, axis, split_axis=0, concat_axis=0, tiled=True)]
    dot_general x13 -> x0, matrix products: 8.97 us -> none  [the longest x1 1.87 us: delta_read(): jnp.einsum('mfd,mdx->mfx', weight_matrix_rows, previous_state, precision=...]
  transfers between devices with their start and end apart: 2 -> 0, of which waited for: 1 -> 0; matrix products, arithmetic and copies ran while one was open for 31% -> 0% of each run, Pallas kernels for 0% -> 0%
where the time goes in v1:
time: 73.9 us; the launch traced here: 73.7 us
  Pallas kernels  72.4 us (98%)
  local copies, waits for them, and re-layouts  1.28 us (2%)
    pallas_call x1, Pallas kernels, local(): pl.pallas_call(kernel, out_shape=jax.ShapeDtypeStruct((4, 512), BF), in_s...  72.4 us

profile of v1, /device:TPU:1, one launch (start us, length us, event | category | flops | bytes accessed | tf_op | source)
XLA Modules:
  0.0 73.7 jit_solution(12962582871288717407)
XLA Ops:
  0.0 72.4 %shard_map.172 = bf16[4,512]{1,0:T(4,128)(2,1)} custom-call(bf16[4,512]{1,0:T(4,128)(2,1)} %bitcast.11, f32[1,32]{1,0:T(1,128)} %bitcast.12, bf16[32,256]{1,0:T(8,128)(2,1)} %wq.1, bf16[32,256]{1,0:T(8,128)(2,1)} %wk.1, bf16[32,256]{1,0:T(8,128)(2,1)} %wv.1, bf16[2,32]{1,0:T(2,128)(2,1)} %bitcast.13, bf16[2,32]{1,0:T(2,128)(2,1)} %bitcast.14, f32[2]{0:T(128)} %rate.1, ...), custom_call_target="tpu_custom_call" | custom-call | tf_op jit(solution)/shard_map/pallas_call | solution.py:341
  72.4 1.3 %copy.20 = bf16[512,4]{0,1:T(4,128)(2,1)} copy(bf16[512,4]{0,1:T(4,128)(2,1)} %bitcast.10) | data formatting | bytes 8192

commit v2 on v1

v2 whole, which is shorter than its diff:
```python
import jax
import jax.numpy as jnp
from jax import lax
from jax.experimental import pallas as pl
from jax.experimental.pallas import tpu as pltpu
from jax.sharding import PartitionSpec as P

D = 2048
N = 8
SEQ = 64
T_LEN = 64
epsilon = 1e-06
BF = jnp.bfloat16
F32 = jnp.float32
HI = lax.Precision.HIGHEST
MESH = pl.DeviceIdType.MESH

(TOK_A, TOK_Y, TOK_Z, W_Y, W_Z, W_B, W_D, G_MIX, G_MIZ, G_MLP, W_OUT, W_UP, W_UP2, W_DOWN, W_DOWN2,
 P_Y, P_Z, P_AUX, HEADS, ATT, U_MAIN, U_AUX, HID, DOWN, FIN) = range(25)
FAR_FIRST = (4, 3, 5, 2, 6, 1, 7)


def nt(a, b, precision=None):
    return lax.dot_general(a, b, (((1,), (1,)), ((), ())), preferred_element_type=F32, precision=precision)


def nn(a, b, precision=None):
    return lax.dot_general(a, b, (((1,), (0,)), ((), ())), preferred_element_type=F32, precision=precision)


def iota(shape, dim):
    return lax.broadcasted_iota(jnp.int32, shape, dim)


def split_rows(x):
    high = x.astype(BF)
    low = (x - high.astype(F32)).astype(BF)
    return jnp.concatenate([high.astype(F32), low.astype(F32)], axis=0).astype(BF)


def own_row(r):
    return jnp.sum(jnp.where(iota(r.shape, 0) == iota(r.shape, 1), r, 0.0), axis=0)


def rows_by(x, mats, contract):
    both = split_rows(x)
    lhs = jnp.broadcast_to(both[None], (N, *both.shape))
    r = lax.dot_general(lhs, mats, (((2,), (contract,)), ((0,), (0,))), preferred_element_type=F32)
    return own_row(r[:, :N] + r[:, N:])


def unit(x):
    return x * lax.rsqrt(jnp.sum(x * x, axis=-1, keepdims=True) + epsilon)


def silu(x):
    return x * (1.0 / (1.0 + jnp.exp(-x)))


def kernel(
    tok, mix_gain, wq, wk, wv, wb, wd, rate, state, tail_k, tail_v, tail_b, tail_g, lengths, wo, mlp_gain, wu, wdn,
    out,
    tok_a, x32, perm, xs, xt, xzs, xzt, xf, gy, gz, gb, gd, ggm, ggz, ggl, go, gu, gdn, dperm, bd, gains,
    kbuf, vbuf, sbuf, sbf, tbb, tgg, tri, coef, pys, pyr, pzs, pzr, pxs, pxr, heads, att, mixed, mixt,
    ums, umr, uxs, uxr, hid, dns, dnr, fins, finr, flat, send_sem, recv_sem, local_sem,
):
    kv = lax.axis_index("kv")
    tp = lax.axis_index("tp")
    z = kv // N
    y = kv % N

    def peer(axis, r):
        if axis == "z":
            return (((z + r) % N) * N + y, tp)
        if axis == "y":
            return (z * N + (y + r) % N, tp)
        return (kv, (tp + r) % N)

    me = {"z": z, "y": y, "tp": tp}
    started = []

    def copy(phase, axis, src, dst, r):
        pltpu.make_async_remote_copy(
            src_ref=src,
            dst_ref=dst,
            send_sem=send_sem.at[phase],
            recv_sem=recv_sem.at[phase],
            device_id=peer(axis, r),
            device_id_type=MESH,
        ).start()

    def gather(phase, axis, buf, steps=FAR_FIRST):
        started.append((phase, buf, len(steps)))
        for r in steps:
            copy(phase, axis, buf.at[me[axis]], buf.at[me[axis]], r)

    def scatter(phase, axis, src, dst):
        started.append((phase, dst, N - 1))
        for r in FAR_FIRST:
            copy(phase, axis, src.at[(me[axis] + r) % N], dst.at[me[axis]], r)

    def relay(phase, axis, buf):
        started.append((phase, buf, 3))
        behind, ahead = (me[axis] + N - 2) % N, (me[axis] + 2) % N
        copy(phase, axis, buf.at[behind], buf.at[behind], 2)
        copy(phase, axis, buf.at[behind], buf.at[behind], 1)
        copy(phase, axis, buf.at[ahead], buf.at[ahead], 7)

    def recv(phase):
        for p, buf, count in started:
            if p == phase:
                part = buf.at[pl.ds(0, count)]
                pltpu.make_async_copy(part, part, recv_sem.at[phase]).wait()

    loads = {}

    def load(name, src, dst):
        c = pltpu.make_async_copy(src, dst, local_sem.at[len(loads)])
        c.start()
        loads[name] = c

    load("tok", tok, tok_a.at[tp])
    load("mix", mix_gain, ggm.at[y])
    load("miz", mix_gain, ggz.at[z])
    load("b", wb, gb.at[y])
    load("d", wd, gd.at[y])
    load("q", wq, gy.at[y, :, pl.ds(0, 256)])
    load("k0", wk.at[:, pl.ds(0, 128)], gy.at[y, :, pl.ds(256, 128)])
    load("k1", wk.at[:, pl.ds(128, 128)], gz.at[z, :, pl.ds(0, 128)])
    load("v", wv, gz.at[z, :, pl.ds(128, 256)])
    load("mlp", mlp_gain, ggl.at[y])
    load("out", wo, go.at[y])
    load("up", wu, gu.at[y])
    load("down", wdn, gdn.at[y])
    load("tb", tail_b, tbb)
    load("tg", tail_g, tgg)
    for h in range(2):
        load(("tk", h), tail_k.at[:, h], kbuf.at[h])
        load(("ts", h), state.at[:, h], sbuf.at[h])
        load(("tv", h), tail_v.at[:, h], vbuf.at[h])

    barrier = pltpu.get_barrier_semaphore()
    for r in FAR_FIRST:
        for axis in ("z", "y", "tp"):
            pl.semaphore_signal(barrier, inc=1, device_id=peer(axis, r), device_id_type=MESH)

    bd[...] = jnp.zeros_like(bd)
    flat[...] = jnp.zeros_like(flat)
    row = iota((N * SEQ, N * SEQ), 0)
    column = iota((N * SEQ, N * SEQ), 1)
    swapped = (row // 64) * 8 + ((row // 8) % 8) * 64 + row % 8
    perm[...] = jnp.where(column == swapped, 1.0, 0.0).astype(BF)
    for name in loads:
        loads[name].wait()

    pl.semaphore_wait(barrier, 3 * (N - 1))

    gather(TOK_A, "tp", tok_a)
    gather(G_MIX, "y", ggm)
    gather(W_B, "y", gb)
    gather(W_D, "y", gd)
    gather(G_MIZ, "z", ggz)
    gather(W_Y, "y", gy)
    gather(W_Z, "z", gz)
    gather(G_MLP, "y", ggl)

    lens = jnp.zeros((N, T_LEN), jnp.int32)
    for i in range(N):
        lens = jnp.where(iota((N, T_LEN), 0) == i, lengths[i], lens)
    live = iota((N, T_LEN), 1) < lens
    upper = jnp.where(iota((T_LEN, T_LEN), 0) <= iota((T_LEN, T_LEN), 1), 1.0, 0.0)
    betas, gammas, totals, b3, g3, c3 = [], [], [], [], [], []
    for h in range(2):
        beta = jnp.where(live, tbb[:, h, :], 0.0)
        decay = jnp.where(live, tgg[:, h, :], 0.0)
        gamma = nn(decay, upper, HI)
        betas.append(beta)
        gammas.append(gamma)
        totals.append(jnp.sum(decay, axis=1, keepdims=True))
        b3.append(beta[:, None, :])
        g3.append(decay[:, None, :])
        c3.append(gamma[:, None, :])
    b3 = jnp.concatenate(b3, axis=0)
    g3 = jnp.concatenate(g3, axis=0)
    c3 = jnp.concatenate(c3, axis=0)
    keys = kbuf[...].reshape(2 * N, T_LEN, 128)
    gram = lax.dot_general(keys, keys, (((2,), (2,)), ((0,), (0,))), preferred_element_type=F32)
    i0 = iota((2 * N, T_LEN, T_LEN), 1)
    j0 = iota((2 * N, T_LEN, T_LEN), 2)
    diagonal = jnp.where(i0 == j0, gram, 0.0)
    inv_row = lax.rsqrt(jnp.sum(diagonal, axis=1, keepdims=True) + epsilon)
    inv_col = lax.rsqrt(jnp.sum(diagonal, axis=2, keepdims=True) + epsilon)
    gamma_col = jnp.sum(jnp.where(j0 <= i0, g3, 0.0), axis=2, keepdims=True)
    beta_col = jnp.sum(jnp.where(j0 == i0, b3, 0.0), axis=2, keepdims=True)
    below = i0 > j0
    lower = jnp.where(
        below, beta_col * jnp.exp(jnp.where(below, gamma_col - c3, 0.0)) * gram * inv_col * inv_row, 0.0
    )
    for n in range(2 * N):
        coef[n : n + 1, :] = inv_row[n]
    tri[...] = lower
    sbf[...] = sbuf[...].astype(BF)

    recv(TOK_A)
    for t in range(N):
        x32[4 * t : 4 * t + 4, :] = tok_a[t].astype(F32)
    whole = x32[...].astype(BF)
    arranged = nn(whole, perm[...])
    for t in range(N):
        xs[t] = arranged[:, 64 * t : 64 * t + 64].astype(BF)
        xzs[t] = x32[:, 64 * t : 64 * t + 64].astype(BF)
    xt[y] = xs[y]
    xzt[z] = xzs[z]
    scatter(TOK_Y, "y", xs, xt)
    scatter(TOK_Z, "z", xzs, xzt)
    gather(W_UP, "y", gu, (2, 6, 1, 7))

    def part(m):
        return jnp.where((i0 // (2 * m) == j0 // (2 * m)) & (i0 // m != j0 // m), tri[...], 0.0)

    def bmm(a, b):
        return lax.dot_general(a, b, (((2,), (1,)), ((0,), (0,))), preferred_element_type=F32, precision=HI)

    inverse = jnp.where(i0 == j0, 1.0, 0.0) - part(1)
    for m in (2, 4, 8, 16, 32):
        inverse = inverse - bmm(bmm(inverse, part(m)), inverse)
    tri[...] = inverse

    for phase in (G_MIX, G_MIZ, W_B, W_D):
        recv(phase)
    for t in range(N):
        gains[0:1, 32 * t : 32 * t + 32] = ggm[t]
        gains[1:2, 32 * t : 32 * t + 32] = ggz[t]
        bd[0:2, 32 * t : 32 * t + 32] = gb[t].astype(F32)
        bd[2:4, 32 * t : 32 * t + 32] = gd[t].astype(F32)
    eye64 = jnp.where(iota((SEQ, SEQ), 0) == iota((SEQ, SEQ), 1), 1.0, 0.0).astype(BF)
    recv(TOK_Y)
    token = nt(eye64, xt[...].reshape(256, SEQ))
    xf[...] = token
    squares = jnp.sum(token * token, axis=1, keepdims=True)
    normed = (token * gains[0:1, :]).astype(BF)
    aux = nt(normed, bd[...].astype(BF))
    pxs[...] = jnp.where(iota((SEQ, 128), 1) == 4, squares, aux).reshape(N, N, 128)
    pxr[z] = pxs[z]
    scatter(P_AUX, "z", pxs, pxr)
    recv(W_Y)
    pys[...] = nn(normed, gy[...].reshape(256, 384)).reshape(N, N, 384).astype(BF)
    pyr[z] = pys[z]
    scatter(P_Y, "z", pys, pyr)
    recv(TOK_Z)
    other = (nt(eye64, xzt[...].reshape(256, SEQ)) * gains[1:2, :]).astype(BF)
    recv(W_Z)
    pzs[...] = nn(other, gz[...].reshape(256, 384)).reshape(N, N, 384).astype(BF)
    pzr[y] = pzs[y]
    scatter(P_Z, "y", pzs, pzr)
    gather(W_OUT, "y", go)
    r0 = iota((256, 256), 0)
    r1 = iota((256, 256), 1)
    regroup = jnp.where(r1 == ((r0 // 4) % 8) * 32 + (r0 // 32) * 4 + r0 % 4, 1.0, 0.0).astype(BF)

    recv(W_UP)
    relay(W_UP2, "y", gu)
    gather(W_DOWN, "y", gdn, (2, 6, 1, 7))
    recv(P_AUX)
    aux = jnp.sum(pxr[...], axis=0)
    row_scale = lax.rsqrt(aux[:, 4:5] / D + epsilon)
    recv(P_Y)
    raw_y = jnp.sum(pyr[...].astype(F32), axis=0) * row_scale
    recv(P_Z)
    raw_z = jnp.sum(pzr[...].astype(F32), axis=0) * row_scale
    results = []
    for h in range(2):
        query = unit(silu(raw_y[:, 128 * h : 128 * h + 128]))
        key = unit(silu(raw_y[:, 256:384] if h == 0 else raw_z[:, 0:128]))
        value = silu(raw_z[:, 128 + 128 * h : 256 + 128 * h])
        new_beta = 1.0 / (1.0 + jnp.exp(-(aux[:, h : h + 1] * row_scale)))
        pre = aux[:, 2 + h : 3 + h] * row_scale
        soft = jnp.maximum(pre, 0.0) + jnp.log(1.0 + jnp.exp(-jnp.abs(pre)))
        new_decay = -rate[h] * soft
        weight = new_beta * jnp.sum(key * query, axis=1, keepdims=True)
        test = query - weight * key
        inv = coef[N * h : N * h + N, :]
        a = rows_by(test, kbuf[h], 2) * jnp.exp(totals[h] - gammas[h]) * inv
        lhs = jnp.broadcast_to(a[None], (N, N, T_LEN))
        solved = own_row(bmm(lhs, tri[N * h : N * h + N])) * betas[h]
        from_values = rows_by(solved, vbuf[h], 1)
        moved = jnp.exp(totals[h]) * test - rows_by(solved * jnp.exp(gammas[h]) * inv, kbuf[h], 1)
        readout = rows_by(moved, sbf[h], 1) + from_values
        results.append(jnp.exp(new_decay) * readout + weight * value)
    heads[z] = jnp.concatenate(results, axis=1).astype(BF)
    gather(HEADS, "z", heads)

    recv(W_OUT)
    recv(G_MLP)
    for t in range(N):
        gains[2:3, 32 * t : 32 * t + 32] = ggl[t]
    recv(HEADS)
    gathered = heads[...].astype(F32).reshape(SEQ, 256).astype(BF)
    att[tp] = nt(gathered, go[...].reshape(256, 256)).astype(BF)
    gather(ATT, "tp", att)
    recv(W_DOWN)
    relay(W_DOWN2, "y", gdn)
    recv(W_UP2)
    recv(ATT)
    mixed[...] = (xf[...] + jnp.sum(att[...].astype(F32), axis=0)).astype(BF)
    mixer = mixed[...].astype(F32)
    normed = (mixer * gains[2:3, :]).astype(BF)
    ums[...] = nn(normed, gu[...].reshape(256, 1024)).reshape(N, N, 1024).astype(BF)
    umr[z] = ums[z]
    scatter(U_MAIN, "z", ums, umr)
    squares = jnp.sum(mixer * mixer, axis=1, keepdims=True)
    uxs[...] = jnp.broadcast_to(squares, (SEQ, 128)).reshape(N, N, 128)
    uxr[z] = uxs[z]
    scatter(U_AUX, "z", uxs, uxr)
    mixt[...] = nt(regroup, mixed[...]).reshape(N, 32, SEQ)
    recv(U_MAIN)
    raw = jnp.sum(umr[...].astype(F32), axis=0)
    recv(U_AUX)
    row_scale = lax.rsqrt(jnp.sum(uxr[...], axis=0)[:, 0:1] / D + epsilon)
    raw = jnp.maximum(raw * row_scale, 0.0)
    hid[z] = (raw * raw).astype(BF)
    gather(HID, "z", hid)
    recv(W_DOWN2)
    dperm[...] = nn(regroup, gdn[...].reshape(256, 1024)).astype(BF)
    recv(HID)
    hidden = hid[...].astype(F32).reshape(SEQ, 1024).astype(BF)
    dns[...] = nt(dperm[...], hidden).reshape(N, 32, SEQ).astype(BF)
    dnr[tp] = dns[tp]
    scatter(DOWN, "tp", dns, dnr)
    recv(DOWN)
    total = mixt[tp] + jnp.sum(dnr[...].astype(F32), axis=0)
    for t in range(N):
        fins[t] = total[4 * t : 4 * t + 4, :].astype(BF)
    finr[y] = fins[y]
    scatter(FIN, "y", fins, finr)
    for phase, buf, count in started[:-1]:
        part_of = buf.at[pl.ds(0, count)]
        pltpu.make_async_copy(part_of, part_of, send_sem.at[phase]).wait()
    recv(FIN)
    for t in range(N):
        flat[0:4, 64 * t : 64 * t + 64] = finr[t].astype(F32)
    out[...] = nn(flat[...].astype(BF), perm[...])[0:4, :].astype(BF)
    last = finr.at[pl.ds(0, N - 1)]
    pltpu.make_async_copy(last, last, send_sem.at[FIN]).wait()


def local(
    tokens, mix_gain, query_weight, key_weight, value_weight, beta_weight, decay_weight, decay_rate, prior_state,
    tail_keys, tail_values, tail_beta, tail_decay, lengths, out_weight, mlp_gain, up_weight, down_weight,
):
    vmem = pl.BlockSpec(memory_space=pltpu.VMEM)
    smem = pl.BlockSpec(memory_space=pltpu.SMEM)
    hbm = pl.BlockSpec(memory_space=pl.ANY)
    specs = [hbm] * 7 + [smem] + [hbm] * 5 + [smem] + [hbm] * 4

    def v(*shape, dtype=BF):
        return pltpu.VMEM(shape, dtype)

    def f(*shape):
        return v(*shape, dtype=F32)

    result = pl.pallas_call(
        kernel,
        out_shape=jax.ShapeDtypeStruct((4, 512), BF),
        in_specs=specs,
        out_specs=vmem,
        scratch_shapes=[
            v(8, 4, 512), f(32, 512), v(512, 512), v(8, 32, 64), v(8, 32, 64), v(8, 32, 64), v(8, 32, 64), f(64, 256),
            v(8, 32, 384), v(8, 32, 384), v(8, 2, 32), v(8, 2, 32), f(8, 1, 32), f(8, 1, 32), f(8, 1, 32),
            v(8, 32, 256), v(8, 32, 1024), v(8, 32, 1024), v(256, 1024), f(128, 256), f(8, 256),
            v(2, 8, 64, 128), v(2, 8, 64, 128), f(2, 8, 128, 128), v(2, 8, 128, 128), f(8, 2, 64), f(8, 2, 64),
            f(16, 64, 64), f(16, 64),
            v(8, 8, 384), v(8, 8, 384), v(8, 8, 384), v(8, 8, 384), f(8, 8, 128), f(8, 8, 128),
            v(8, 8, 256), v(8, 64, 256), v(64, 256), f(8, 32, 64),
            v(8, 8, 1024), v(8, 8, 1024), f(8, 8, 128), f(8, 8, 128),
            v(8, 8, 1024), v(8, 32, 64), v(8, 32, 64), v(8, 4, 64), v(8, 4, 64), f(8, 512),
            pltpu.SemaphoreType.DMA((25,)), pltpu.SemaphoreType.DMA((25,)), pltpu.SemaphoreType.DMA((21,)),
        ],
        compiler_params=pltpu.CompilerParams(collective_id=0, has_side_effects=True),
    )(
        tokens.T, mix_gain.reshape(1, -1), query_weight, key_weight, value_weight, beta_weight.T, decay_weight.T,
        decay_rate, prior_state, tail_keys, tail_values, tail_beta, tail_decay, lengths, out_weight.T,
        mlp_gain.reshape(1, -1), up_weight, down_weight.T,
    )
    return result.T


def solution(mesh):
    kt = ("kv", "tp")
    return jax.shard_map(
        local,
        mesh=mesh,
        in_specs=(
            P(None, kt), P("kv"), P("kv", "tp"), P("kv", "tp"), P("kv", "tp"), P("kv", "tp"), P("kv", "tp"), P("tp"),
            P("kv", "tp", None, None), P("kv", "tp", None, None), P("kv", "tp", None, None),
            P("kv", "tp", None), P("kv", "tp", None), P("kv"), P("tp", "kv"), P("kv"), P("kv", "tp"), P("tp", "kv"),
        ),
        out_specs=P(None, kt),
        check_vma=False,
    )
```

time: 73.9 us -> 65.3 us (0.88)
  Pallas kernels: 72.4 us -> 63.9 us
    pallas_call x1, Pallas kernels: 72.4 us -> 63.9 us  [local(): pl.pallas_call(kernel, out_shape=jax.ShapeDtypeStruct((4, 512), BF), in_s...]
where the time goes in v2:
time: 65.3 us; the launch traced here: 65.2 us
  Pallas kernels  63.9 us (98%)
  local copies, waits for them, and re-layouts  1.28 us (2%)
    pallas_call x1, Pallas kernels, local(): pl.pallas_call(kernel, out_shape=jax.ShapeDtypeStruct((4, 512), BF), in_s...  63.9 us

profile of v2, /device:TPU:1, one launch (start us, length us, event | category | flops | bytes accessed | tf_op | source)
XLA Modules:
  0.0 65.2 jit_solution(18393139746122490408)
XLA Ops:
  0.0 63.9 %shard_map.172 = bf16[4,512]{1,0:T(4,128)(2,1)} custom-call(bf16[4,512]{1,0:T(4,128)(2,1)} %bitcast.11, f32[1,32]{1,0:T(1,128)} %bitcast.12, bf16[32,256]{1,0:T(8,128)(2,1)} %wq.1, bf16[32,256]{1,0:T(8,128)(2,1)} %wk.1, bf16[32,256]{1,0:T(8,128)(2,1)} %wv.1, bf16[2,32]{1,0:T(2,128)(2,1)} %bitcast.13, bf16[2,32]{1,0:T(2,128)(2,1)} %bitcast.14, f32[2]{0:T(128)} %rate.1, ...), custom_call_target="tpu_custom_call" | custom-call | tf_op jit(solution)/shard_map/pallas_call | solution.py:362
  63.9 1.3 %copy.20 = bf16[512,4]{0,1:T(4,128)(2,1)} copy(bf16[512,4]{0,1:T(4,128)(2,1)} %bitcast.10) | data formatting | bytes 8192

commit v3 on v2

--- a/solution.py
+++ b/solution.py
@@ -15,8 +15,8 @@
 HI = lax.Precision.HIGHEST
 MESH = pl.DeviceIdType.MESH
 
-(TOK_A, TOK_Y, TOK_Z, W_Y, W_Z, W_B, W_D, G_MIX, G_MIZ, G_MLP, W_OUT, W_UP, W_UP2, W_DOWN, W_DOWN2,
- P_Y, P_Z, P_AUX, HEADS, ATT, U_MAIN, U_AUX, HID, DOWN, FIN) = range(25)
+(TOK_A, TOK_Y, TOK_Z, W_Y, W_Z, W_B, W_D, G_MIX, G_MIZ, G_MLP, W_OUT, W_OUT2, W_UP, W_UP2, W_DOWN, W_DOWN2,
+ P_Y, P_Z, HEADS, ATT, U_MAIN, HID, DOWN) = range(23)
 FAR_FIRST = (4, 3, 5, 2, 6, 1, 7)
 
 
@@ -60,9 +60,9 @@
 def kernel(
     tok, mix_gain, wq, wk, wv, wb, wd, rate, state, tail_k, tail_v, tail_b, tail_g, lengths, wo, mlp_gain, wu, wdn,
     out,
-    tok_a, x32, perm, xs, xt, xzs, xzt, xf, gy, gz, gb, gd, ggm, ggz, ggl, go, gu, gdn, dperm, bd, gains,
-    kbuf, vbuf, sbuf, sbf, tbb, tgg, tri, coef, pys, pyr, pzs, pzr, pxs, pxr, heads, att, mixed, mixt,
-    ums, umr, uxs, uxr, hid, dns, dnr, fins, finr, flat, send_sem, recv_sem, local_sem,
+    tok_a, x32, perm, xs, xt, xzs, xzt, xf, gy, gz, gb, gd, ggm, ggz, ggl, go, gu, gdn, bd, gains,
+    kbuf, vbuf, sbuf, sbf, tbb, tgg, tri, coef, pys, pyr, pzs, pzr, heads, att, mixed, mixt,
+    ums, umr, hid, down_t, dns, dnr, flat, send_sem, recv_sem, local_sem,
 ):
     kv = lax.axis_index("kv")
     tp = lax.axis_index("tp")
@@ -111,6 +111,11 @@
             if p == phase:
                 part = buf.at[pl.ds(0, count)]
                 pltpu.make_async_copy(part, part, recv_sem.at[phase]).wait()
+
+    barrier = pltpu.get_barrier_semaphore()
+    for r in FAR_FIRST:
+        for axis in ("z", "y", "tp"):
+            pl.semaphore_signal(barrier, inc=1, device_id=peer(axis, r), device_id_type=MESH)
 
     loads = {}
 
@@ -139,23 +144,13 @@
         load(("ts", h), state.at[:, h], sbuf.at[h])
         load(("tv", h), tail_v.at[:, h], vbuf.at[h])
 
-    barrier = pltpu.get_barrier_semaphore()
-    for r in FAR_FIRST:
-        for axis in ("z", "y", "tp"):
-            pl.semaphore_signal(barrier, inc=1, device_id=peer(axis, r), device_id_type=MESH)
-
-    bd[...] = jnp.zeros_like(bd)
-    flat[...] = jnp.zeros_like(flat)
-    row = iota((N * SEQ, N * SEQ), 0)
-    column = iota((N * SEQ, N * SEQ), 1)
-    swapped = (row // 64) * 8 + ((row // 8) % 8) * 64 + row % 8
-    perm[...] = jnp.where(column == swapped, 1.0, 0.0).astype(BF)
-    for name in loads:
-        loads[name].wait()
+    loads.pop("tok").wait()
 
     pl.semaphore_wait(barrier, 3 * (N - 1))
 
     gather(TOK_A, "tp", tok_a)
+    for name in ("mix", "miz", "b", "d", "q", "k0", "k1", "v", "mlp", "out"):
+        loads.pop(name).wait()
     gather(G_MIX, "y", ggm)
     gather(W_B, "y", gb)
     gather(W_D, "y", gd)
@@ -163,7 +158,16 @@
     gather(W_Y, "y", gy)
     gather(W_Z, "z", gz)
     gather(G_MLP, "y", ggl)
-
+    gather(W_OUT, "y", go, (2, 6, 1, 7))
+    for name in loads:
+        loads[name].wait()
+
+    bd[...] = jnp.zeros_like(bd)
+    flat[...] = jnp.zeros_like(flat)
+    row = iota((N * SEQ, N * SEQ), 0)
+    column = iota((N * SEQ, N * SEQ), 1)
+    swapped = (row // 64) * 8 + ((row // 8) % 8) * 64 + row % 8
+    perm[...] = jnp.where(column == swapped, 1.0, 0.0).astype(BF)
     lens = jnp.zeros((N, T_LEN), jnp.int32)
     for i in range(N):
         lens = jnp.where(iota((N, T_LEN), 0) == i, lengths[i], lens)
@@ -215,17 +219,6 @@
     scatter(TOK_Z, "z", xzs, xzt)
     gather(W_UP, "y", gu, (2, 6, 1, 7))
 
-    def part(m):
-        return jnp.where((i0 // (2 * m) == j0 // (2 * m)) & (i0 // m != j0 // m), tri[...], 0.0)
-
-    def bmm(a, b):
-        return lax.dot_general(a, b, (((2,), (1,)), ((0,), (0,))), preferred_element_type=F32, precision=HI)
-
-    inverse = jnp.where(i0 == j0, 1.0, 0.0) - part(1)
-    for m in (2, 4, 8, 16, 32):
-        inverse = inverse - bmm(bmm(inverse, part(m)), inverse)
-    tri[...] = inverse
-
     for phase in (G_MIX, G_MIZ, W_B, W_D):
         recv(phase)
     for t in range(N):
@@ -240,11 +233,13 @@
     squares = jnp.sum(token * token, axis=1, keepdims=True)
     normed = (token * gains[0:1, :]).astype(BF)
     aux = nt(normed, bd[...].astype(BF))
-    pxs[...] = jnp.where(iota((SEQ, 128), 1) == 4, squares, aux).reshape(N, N, 128)
-    pxr[z] = pxs[z]
-    scatter(P_AUX, "z", pxs, pxr)
+    lane = iota((SEQ, 128), 1)
+    aux = jnp.where(lane == 4, squares, aux)
+    high = aux.astype(BF).astype(F32)
+    aux = jnp.where(lane < 64, high, pltpu.roll(aux - high, 64, 1))
+    pys[:, :, 384:512] = aux.reshape(N, N, 128).astype(BF)
     recv(W_Y)
-    pys[...] = nn(normed, gy[...].reshape(256, 384)).reshape(N, N, 384).astype(BF)
+    pys[:, :, 0:384] = nn(normed, gy[...].reshape(256, 384)).reshape(N, N, 384).astype(BF)
     pyr[z] = pys[z]
     scatter(P_Y, "z", pys, pyr)
     recv(TOK_Z)
@@ -253,19 +248,32 @@
     pzs[...] = nn(other, gz[...].reshape(256, 384)).reshape(N, N, 384).astype(BF)
     pzr[y] = pzs[y]
     scatter(P_Z, "y", pzs, pzr)
-    gather(W_OUT, "y", go)
+    recv(W_OUT)
+    relay(W_OUT2, "y", go)
     r0 = iota((256, 256), 0)
     r1 = iota((256, 256), 1)
-    regroup = jnp.where(r1 == ((r0 // 4) % 8) * 32 + (r0 // 32) * 4 + r0 % 4, 1.0, 0.0).astype(BF)
+    turn = jnp.where((r0 == r1) & ((r0 // 4) % N == tp), 1.0, 0.0).astype(BF)
+
+    def part(m):
+        return jnp.where((i0 // (2 * m) == j0 // (2 * m)) & (i0 // m != j0 // m), tri[...], 0.0)
+
+    def bmm(a, b):
+        return lax.dot_general(a, b, (((2,), (1,)), ((0,), (0,))), preferred_element_type=F32, precision=HI)
+
+    inverse = jnp.where(i0 == j0, 1.0, 0.0) - part(1)
+    for m in (2, 4, 8, 16, 32):
+        inverse = inverse - bmm(bmm(inverse, part(m)), inverse)
+    tri[...] = inverse
 
     recv(W_UP)
     relay(W_UP2, "y", gu)
     gather(W_DOWN, "y", gdn, (2, 6, 1, 7))
-    recv(P_AUX)
-    aux = jnp.sum(pxr[...], axis=0)
+    recv(P_Y)
+    raw_y = jnp.sum(pyr[...].astype(F32), axis=0)
+    aux = raw_y[:, 384:512]
+    aux = aux + pltpu.roll(aux, 64, 1)
     row_scale = lax.rsqrt(aux[:, 4:5] / D + epsilon)
-    recv(P_Y)
-    raw_y = jnp.sum(pyr[...].astype(F32), axis=0) * row_scale
+    raw_y = raw_y * row_scale
     recv(P_Z)
     raw_z = jnp.sum(pzr[...].astype(F32), axis=0) * row_scale
     results = []
@@ -290,7 +298,7 @@
     heads[z] = jnp.concatenate(results, axis=1).astype(BF)
     gather(HEADS, "z", heads)
 
-    recv(W_OUT)
+    recv(W_OUT2)
     recv(G_MLP)
     for t in range(N):
         gains[2:3, 32 * t : 32 * t + 32] = ggl[t]
@@ -298,50 +306,55 @@
     gathered = heads[...].astype(F32).reshape(SEQ, 256).astype(BF)
     att[tp] = nt(gathered, go[...].reshape(256, 256)).astype(BF)
     gather(ATT, "tp", att)
-    recv(W_DOWN)
-    relay(W_DOWN2, "y", gdn)
     recv(W_UP2)
     recv(ATT)
     mixed[...] = (xf[...] + jnp.sum(att[...].astype(F32), axis=0)).astype(BF)
     mixer = mixed[...].astype(F32)
     normed = (mixer * gains[2:3, :]).astype(BF)
-    ums[...] = nn(normed, gu[...].reshape(256, 1024)).reshape(N, N, 1024).astype(BF)
+    ums[:, :, 0:1024] = nn(normed, gu[...].reshape(256, 1024)).reshape(N, N, 1024).astype(BF)
+    squares = jnp.sum(mixer * mixer, axis=1, keepdims=True)
+    high = squares.astype(BF).astype(F32)
+    ums[:, :, 1024:1152] = jnp.where(lane < 64, high, squares - high).reshape(N, N, 128).astype(BF)
     umr[z] = ums[z]
     scatter(U_MAIN, "z", ums, umr)
-    squares = jnp.sum(mixer * mixer, axis=1, keepdims=True)
-    uxs[...] = jnp.broadcast_to(squares, (SEQ, 128)).reshape(N, N, 128)
-    uxr[z] = uxs[z]
-    scatter(U_AUX, "z", uxs, uxr)
-    mixt[...] = nt(regroup, mixed[...]).reshape(N, 32, SEQ)
+    recv(W_DOWN)
+    relay(W_DOWN2, "y", gdn)
+    mixt[...] = nt(turn, mixed[...])
     recv(U_MAIN)
     raw = jnp.sum(umr[...].astype(F32), axis=0)
-    recv(U_AUX)
-    row_scale = lax.rsqrt(jnp.sum(uxr[...], axis=0)[:, 0:1] / D + epsilon)
-    raw = jnp.maximum(raw * row_scale, 0.0)
+    row_scale = lax.rsqrt((raw[:, 1024:1025] + raw[:, 1088:1089]) / D + epsilon)
+    raw = jnp.maximum(raw[:, 0:1024] * row_scale, 0.0)
     hid[z] = (raw * raw).astype(BF)
     gather(HID, "z", hid)
     recv(W_DOWN2)
-    dperm[...] = nn(regroup, gdn[...].reshape(256, 1024)).astype(BF)
     recv(HID)
     hidden = hid[...].astype(F32).reshape(SEQ, 1024).astype(BF)
-    dns[...] = nt(dperm[...], hidden).reshape(N, 32, SEQ).astype(BF)
-    dnr[tp] = dns[tp]
-    scatter(DOWN, "tp", dns, dnr)
-    recv(DOWN)
-    total = mixt[tp] + jnp.sum(dnr[...].astype(F32), axis=0)
-    for t in range(N):
-        fins[t] = total[4 * t : 4 * t + 4, :].astype(BF)
-    finr[y] = fins[y]
-    scatter(FIN, "y", fins, finr)
-    for phase, buf, count in started[:-1]:
+    down_t[...] = nt(gdn[...].reshape(256, 1024), hidden) + mixt[...]
+    for t in range(N * N):
+        dns[t] = down_t[4 * t : 4 * t + 4, :].astype(BF)
+    for a in (4, 3, 5, 2, 6, 1, 7, 0):
+        for b in (4, 3, 5, 2, 6, 1, 7, 0):
+            if a or b:
+                to_y, to_tp = (y + a) % N, (tp + b) % N
+                pltpu.make_async_remote_copy(
+                    src_ref=dns.at[to_y * N + to_tp],
+                    dst_ref=dnr.at[y * N + tp],
+                    send_sem=send_sem.at[DOWN],
+                    recv_sem=recv_sem.at[DOWN],
+                    device_id=(z * N + to_y, to_tp),
+                    device_id_type=MESH,
+                ).start()
+    dnr[y * N + tp] = dns[y * N + tp]
+    for phase, buf, count in started:
         part_of = buf.at[pl.ds(0, count)]
         pltpu.make_async_copy(part_of, part_of, send_sem.at[phase]).wait()
-    recv(FIN)
+    others = dnr.at[pl.ds(0, N * N - 1)]
+    pltpu.make_async_copy(others, others, recv_sem.at[DOWN]).wait()
     for t in range(N):
-        flat[0:4, 64 * t : 64 * t + 64] = finr[t].astype(F32)
+        block = jnp.sum(dnr[N * t : N * t + N].astype(F32), axis=0)
+        flat[0:4, 64 * t : 64 * t + 64] = block
     out[...] = nn(flat[...].astype(BF), perm[...])[0:4, :].astype(BF)
-    last = finr.at[pl.ds(0, N - 1)]
-    pltpu.make_async_copy(last, last, send_sem.at[FIN]).wait()
+    pltpu.make_async_copy(others, others, send_sem.at[DOWN]).wait()
 
 
 def local(
@@ -367,14 +380,14 @@
         scratch_shapes=[
             v(8, 4, 512), f(32, 512), v(512, 512), v(8, 32, 64), v(8, 32, 64), v(8, 32, 64), v(8, 32, 64), f(64, 256),
             v(8, 32, 384), v(8, 32, 384), v(8, 2, 32), v(8, 2, 32), f(8, 1, 32), f(8, 1, 32), f(8, 1, 32),
-            v(8, 32, 256), v(8, 32, 1024), v(8, 32, 1024), v(256, 1024), f(128, 256), f(8, 256),
+            v(8, 32, 256), v(8, 32, 1024), v(8, 32, 1024), f(128, 256), f(8, 256),
             v(2, 8, 64, 128), v(2, 8, 64, 128), f(2, 8, 128, 128), v(2, 8, 128, 128), f(8, 2, 64), f(8, 2, 64),
             f(16, 64, 64), f(16, 64),
-            v(8, 8, 384), v(8, 8, 384), v(8, 8, 384), v(8, 8, 384), f(8, 8, 128), f(8, 8, 128),
-            v(8, 8, 256), v(8, 64, 256), v(64, 256), f(8, 32, 64),
-            v(8, 8, 1024), v(8, 8, 1024), f(8, 8, 128), f(8, 8, 128),
-            v(8, 8, 1024), v(8, 32, 64), v(8, 32, 64), v(8, 4, 64), v(8, 4, 64), f(8, 512),
-            pltpu.SemaphoreType.DMA((25,)), pltpu.SemaphoreType.DMA((25,)), pltpu.SemaphoreType.DMA((21,)),
+            v(8, 8, 512), v(8, 8, 512), v(8, 8, 384), v(8, 8, 384),
+            v(8, 8, 256), v(8, 64, 256), v(64, 256), f(256, 64),
+            v(8, 8, 1152), v(8, 8, 1152),
+            v(8, 8, 1024), f(256, 64), v(64, 4, 64), v(64, 4, 64), f(8, 512),
+            pltpu.SemaphoreType.DMA((23,)), pltpu.SemaphoreType.DMA((23,)), pltpu.SemaphoreType.DMA((21,)),
         ],
         compiler_params=pltpu.CompilerParams(collective_id=0, has_side_effects=True),
     )(

time: 65.3 us -> 63.4 us (0.971)
  Pallas kernels: 63.9 us -> 61.9 us
    pallas_call x1, Pallas kernels: 63.9 us -> 61.9 us  [local(): pl.pallas_call(kernel, out_shape=jax.ShapeDtypeStruct((4, 512), BF), in_s...]
where the time goes in v3:
time: 63.4 us; the launch traced here: 63.2 us
  Pallas kernels  61.9 us (98%)
  local copies, waits for them, and re-layouts  1.28 us (2%)
    pallas_call x1, Pallas kernels, local(): pl.pallas_call(kernel, out_shape=jax.ShapeDtypeStruct((4, 512), BF), in_s...  61.9 us
    unnamed x1, local copies, waits for them, and re-layouts  1.28 us

profile of v3, /device:TPU:1, one launch (start us, length us, event | category | flops | bytes accessed | tf_op | source)
XLA Modules:
  0.0 63.2 jit_solution(14181591536722893503)
XLA Ops:
  0.0 61.9 %shard_map.172 = bf16[4,512]{1,0:T(4,128)(2,1)} custom-call(bf16[4,512]{1,0:T(4,128)(2,1)} %bitcast.11, f32[1,32]{1,0:T(1,128)} %bitcast.12, bf16[32,256]{1,0:T(8,128)(2,1)} %wq.1, bf16[32,256]{1,0:T(8,128)(2,1)} %wk.1, bf16[32,256]{1,0:T(8,128)(2,1)} %wv.1, bf16[2,32]{1,0:T(2,128)(2,1)} %bitcast.13, bf16[2,32]{1,0:T(2,128)(2,1)} %bitcast.14, f32[2]{0:T(128)} %rate.1, ...), custom_call_target="tpu_custom_call" | custom-call | tf_op jit(solution)/shard_map/pallas_call | solution.py:375
  62.0 1.3 %copy.20 = bf16[512,4]{0,1:T(4,128)(2,1)} copy(bf16[512,4]{0,1:T(4,128)(2,1)} %bitcast.10) | data formatting | bytes 8192

commit v4 on v3

--- a/solution.py
+++ b/solution.py
@@ -58,11 +58,11 @@
 
 
 def kernel(
-    tok, mix_gain, wq, wk, wv, wb, wd, rate, state, tail_k, tail_v, tail_b, tail_g, lengths, wo, mlp_gain, wu, wdn,
+    tok, mix_gain, wq, wk, wv, wb, wd, rate_in, state, tail_k, tail_v, tail_b, tail_g, lengths_in, wo, mlp_gain, wu, wdn,
     out,
     tok_a, x32, perm, xs, xt, xzs, xzt, xf, gy, gz, gb, gd, ggm, ggz, ggl, go, gu, gdn, bd, gains,
     kbuf, vbuf, sbuf, sbf, tbb, tgg, tri, coef, pys, pyr, pzs, pzr, heads, att, mixed, mixt,
-    ums, umr, hid, down_t, dns, dnr, flat, send_sem, recv_sem, local_sem,
+    ums, umr, hid, down_t, dns, dnr, flat, lengths, rate, send_sem, recv_sem, local_sem,
 ):
     kv = lax.axis_index("kv")
     tp = lax.axis_index("tp")
@@ -137,6 +137,8 @@
     load("out", wo, go.at[y])
     load("up", wu, gu.at[y])
     load("down", wdn, gdn.at[y])
+    load("lengths", lengths_in, lengths)
+    load("rate", rate_in, rate)
     load("tb", tail_b, tbb)
     load("tg", tail_g, tgg)
     for h in range(2):
@@ -362,9 +364,8 @@
     tail_keys, tail_values, tail_beta, tail_decay, lengths, out_weight, mlp_gain, up_weight, down_weight,
 ):
     vmem = pl.BlockSpec(memory_space=pltpu.VMEM)
-    smem = pl.BlockSpec(memory_space=pltpu.SMEM)
     hbm = pl.BlockSpec(memory_space=pl.ANY)
-    specs = [hbm] * 7 + [smem] + [hbm] * 5 + [smem] + [hbm] * 4
+    specs = [hbm] * 18
 
     def v(*shape, dtype=BF):
         return pltpu.VMEM(shape, dtype)
@@ -387,7 +388,8 @@
             v(8, 8, 256), v(8, 64, 256), v(64, 256), f(256, 64),
             v(8, 8, 1152), v(8, 8, 1152),
             v(8, 8, 1024), f(256, 64), v(64, 4, 64), v(64, 4, 64), f(8, 512),
-            pltpu.SemaphoreType.DMA((23,)), pltpu.SemaphoreType.DMA((23,)), pltpu.SemaphoreType.DMA((21,)),
+            pltpu.SMEM((8,), jnp.int32), pltpu.SMEM((2,), F32),
+            pltpu.SemaphoreType.DMA((23,)), pltpu.SemaphoreType.DMA((23,)), pltpu.SemaphoreType.DMA((23,)),
         ],
         compiler_params=pltpu.CompilerParams(collective_id=0, has_side_effects=True),
     )(

time: 63.4 us -> 62.8 us (level)
    pallas_call x1, Pallas kernels: 61.9 us -> 61.3 us  [local(): pl.pallas_call(kernel, out_shape=jax.ShapeDtypeStruct((4, 512), BF), in_s...]
where the time goes in v4:
time: 62.8 us; the launch traced here: 62.6 us
  Pallas kernels  61.3 us (98%)
  local copies, waits for them, and re-layouts  1.28 us (2%)
    pallas_call x1, Pallas kernels, local(): pl.pallas_call(kernel, out_shape=jax.ShapeDtypeStruct((4, 512), BF), in_s...  61.3 us
    unnamed x1, local copies, waits for them, and re-layouts  1.28 us

profile of v4, /device:TPU:1, one launch (start us, length us, event | category | flops | bytes accessed | tf_op | source)
XLA Modules:
  0.0 62.6 jit_solution(7114668787377209489)
XLA Ops:
  0.0 61.3 %shard_map.172 = bf16[4,512]{1,0:T(4,128)(2,1)} custom-call(bf16[4,512]{1,0:T(4,128)(2,1)} %bitcast.11, f32[1,32]{1,0:T(1,128)} %bitcast.12, bf16[32,256]{1,0:T(8,128)(2,1)} %wq.1, bf16[32,256]{1,0:T(8,128)(2,1)} %wk.1, bf16[32,256]{1,0:T(8,128)(2,1)} %wv.1, bf16[2,32]{1,0:T(2,128)(2,1)} %bitcast.13, bf16[2,32]{1,0:T(2,128)(2,1)} %bitcast.14, f32[2]{0:T(128)} %rate_in.1, ...), custom_call_target="tpu_custom_call" | custom-call | tf_op jit(solution)/shard_map/pallas_call | solution.py:376
  61.3 1.3 %copy.20 = bf16[512,4]{0,1:T(4,128)(2,1)} copy(bf16[512,4]{0,1:T(4,128)(2,1)} %bitcast.10) | data formatting | bytes 8192

commit v5 on v4

--- a/solution.py
+++ b/solution.py
@@ -278,25 +278,30 @@
     raw_y = raw_y * row_scale
     recv(P_Z)
     raw_z = jnp.sum(pzr[...].astype(F32), axis=0) * row_scale
-    results = []
-    for h in range(2):
+    both = range(2)
+    tests, weights, invs = [], [], []
+    for h in both:
         query = unit(silu(raw_y[:, 128 * h : 128 * h + 128]))
         key = unit(silu(raw_y[:, 256:384] if h == 0 else raw_z[:, 0:128]))
+        weight = (1.0 / (1.0 + jnp.exp(-(aux[:, h : h + 1] * row_scale)))) * jnp.sum(key * query, axis=1, keepdims=True)
+        tests.append(query - weight * key)
+        weights.append(weight)
+        invs.append(coef[N * h : N * h + N, :])
+    scores = [rows_by(tests[h], kbuf[h], 2) * jnp.exp(totals[h] - gammas[h]) * invs[h] for h in both]
+    solved = [
+        own_row(bmm(jnp.broadcast_to(scores[h][None], (N, N, T_LEN)), tri[N * h : N * h + N])) * betas[h] for h in both
+    ]
+    taken = [rows_by(solved[h] * jnp.exp(gammas[h]) * invs[h], kbuf[h], 1) for h in both]
+    moved = [jnp.exp(totals[h]) * tests[h] - taken[h] for h in both]
+    from_state = [rows_by(moved[h], sbf[h], 1) for h in both]
+    from_values = [rows_by(solved[h], vbuf[h], 1) for h in both]
+    results = []
+    for h in both:
         value = silu(raw_z[:, 128 + 128 * h : 256 + 128 * h])
-        new_beta = 1.0 / (1.0 + jnp.exp(-(aux[:, h : h + 1] * row_scale)))
         pre = aux[:, 2 + h : 3 + h] * row_scale
         soft = jnp.maximum(pre, 0.0) + jnp.log(1.0 + jnp.exp(-jnp.abs(pre)))
-        new_decay = -rate[h] * soft
-        weight = new_beta * jnp.sum(key * query, axis=1, keepdims=True)
-        test = query - weight * key
-        inv = coef[N * h : N * h + N, :]
-        a = rows_by(test, kbuf[h], 2) * jnp.exp(totals[h] - gammas[h]) * inv
-        lhs = jnp.broadcast_to(a[None], (N, N, T_LEN))
-        solved = own_row(bmm(lhs, tri[N * h : N * h + N])) * betas[h]
-        from_values = rows_by(solved, vbuf[h], 1)
-        moved = jnp.exp(totals[h]) * test - rows_by(solved * jnp.exp(gammas[h]) * inv, kbuf[h], 1)
-        readout = rows_by(moved, sbf[h], 1) + from_values
-        results.append(jnp.exp(new_decay) * readout + weight * value)
+        fade = jnp.exp(-rate[h] * soft)
+        results.append(fade * (from_state[h] + from_values[h]) + weights[h] * value)
     heads[z] = jnp.concatenate(results, axis=1).astype(BF)
     gather(HEADS, "z", heads)
 

time: 62.8 us -> 62.2 us (level)
  no operation moved by 1% of the time
where the time goes in v5:
time: 62.2 us; the launch traced here: 62.1 us
  Pallas kernels  60.8 us (98%)
  local copies, waits for them, and re-layouts  1.28 us (2%)
    pallas_call x1, Pallas kernels, local(): pl.pallas_call(kernel, out_shape=jax.ShapeDtypeStruct((4, 512), BF), in_s...  60.8 us
    unnamed x1, local copies, waits for them, and re-layouts  1.28 us

profile of v5, /device:TPU:1, one launch (start us, length us, event | category | flops | bytes accessed | tf_op | source)
XLA Modules:
  0.0 62.1 jit_solution(12175910471639444850)
XLA Ops:
  0.0 60.8 %shard_map.172 = bf16[4,512]{1,0:T(4,128)(2,1)} custom-call(bf16[4,512]{1,0:T(4,128)(2,1)} %bitcast.11, f32[1,32]{1,0:T(1,128)} %bitcast.12, bf16[32,256]{1,0:T(8,128)(2,1)} %wq.1, bf16[32,256]{1,0:T(8,128)(2,1)} %wk.1, bf16[32,256]{1,0:T(8,128)(2,1)} %wv.1, bf16[2,32]{1,0:T(2,128)(2,1)} %bitcast.13, bf16[2,32]{1,0:T(2,128)(2,1)} %bitcast.14, f32[2]{0:T(128)} %rate_in.1, ...), custom_call_target="tpu_custom_call" | custom-call | tf_op jit(solution)/shard_map/pallas_call | solution.py:381
  60.8 1.3 %copy.20 = bf16[512,4]{0,1:T(4,128)(2,1)} copy(bf16[512,4]{0,1:T(4,128)(2,1)} %bitcast.10) | data formatting | bytes 8192
